TPU v7x, 512 devices: a whole 4x4x16 slice. The times are simulated.
512 devices in a mesh: rep: 2 (over z_hi), fs: 32 (over z_lo, y), tp: 8 (over x, core).
Axes of the slice: x: 4, y: 4, z: 16 (z_hi: 2, z_lo: 8; z = z_hi * 8 + z_lo), core: 2. Of those that a mesh axis runs over, the one named last changes fastest.
Arguments:
- tokens: bfloat16 [49152, 2048], P(('rep', 'fs', 'tp')), may hold values from -6 to 6
- norm_gain: float32 [2048], replicated, may hold values from 0.1 to 1.9
- gate_weight: float32 [2048, 5632], P('fs', 'tp'), may hold values from -0.125 to 0.125
- up_weight: float32 [2048, 5632], P('fs', 'tp'), may hold values from -0.125 to 0.125
- gate_scale: float32 [5632], P('tp'), may hold values from 0.3 to 3
- up_scale: float32 [5632], P('tp'), may hold values from 0.3 to 3
- down_weight: float32 [5632, 2048], P('tp', 'fs'), may hold values from -0.078125 to 0.078125
- down_scale: float32 [2048], replicated, may hold values from 0.3 to 3
Outputs:
- mixed: bfloat16 [49152, 2048], P(('rep', 'fs', 'tp'))
All inputs are finite; a program needn't handle non-finite values.
Results may differ from a plain program's by a relative error of at most 0.014.
Values may be sent and summed in bfloat16 or wider, within the bound.
A program may use at most 64 MiB of HBM per device.

v0:
```python
import jax
import jax.numpy as jnp
from jax import lax
from jax.sharding import PartitionSpec as P


def joined_along(blocks, dim):
    shape = list(blocks.shape[1:])
    shape[dim] *= blocks.shape[0]
    return jnp.moveaxis(blocks, 0, dim).reshape(shape)


def sent_to_all(shard, axis):
    size = lax.axis_size(axis)
    return lax.all_to_all(
        jnp.broadcast_to(shard[None], (size, *shard.shape)), axis, 0, 0, tiled=True
    )


def gather_directly(shard, axis, dim):
    return joined_along(sent_to_all(shard, axis), dim)


def in_one_piece(arrays, axis, dim, along):
    both = jnp.concatenate(arrays, axis=along)
    out, at, gathered = (lax.all_gather(both, axis, axis=dim, tiled=True), 0, [])
    for a in arrays:
        gathered.append(lax.slice_in_dim(out, at, at + a.shape[along], axis=along))
        at += a.shape[along]
    return tuple(gathered)


def cut_along(shard, dim, size):
    shape = shard.shape
    blocks = shard.reshape(*shape[:dim], size, shape[dim] // size, *shape[dim + 1 :])
    return jnp.moveaxis(blocks, dim, 0)


def sum_at_owner(shard, axis, dim):
    size = lax.axis_size(axis)
    blocks = lax.all_to_all(cut_along(shard, dim, size), axis, 0, 0, tiled=True)
    return jnp.sum(blocks.astype(jnp.float32), axis=0)


def on_device(
    tokens, norm_gain, gate_weight, up_weight, gate_scale, up_scale, down_weight, down_scale
):
    values = tokens.astype(jnp.float32)
    own_normed = (
        values * lax.rsqrt(jnp.mean(values * values, axis=-1, keepdims=True) + 1e-06) * norm_gain
    ).astype(jnp.bfloat16)
    normed = gather_directly(own_normed, "tp", 0)
    gate_local = gate_weight.astype(jnp.bfloat16)
    up_local = up_weight.astype(jnp.bfloat16)
    gate_whole, up_whole = in_one_piece((gate_local, up_local), "fs", 0, 1)
    gate_value = jnp.dot(normed, gate_whole, preferred_element_type=jnp.float32)
    up_value = jnp.dot(normed, up_whole, preferred_element_type=jnp.float32)
    hidden = (jax.nn.silu(gate_value * gate_scale) * (up_value * up_scale)).astype(jnp.bfloat16)
    partial_value = jnp.dot(
        hidden,
        lax.all_gather(down_weight.astype(jnp.bfloat16), "fs", axis=1, tiled=True),
        preferred_element_type=jnp.float32,
    )
    partial_value = partial_value.astype(jnp.bfloat16).astype(jnp.float32)
    summed = sum_at_owner(partial_value.astype(jnp.bfloat16), "tp", 0)
    return (summed * down_scale).astype(jnp.bfloat16)


def solution(mesh):
    placed = (
        P(("rep", "fs", "tp"), None),
        P(),
        P("fs", "tp"),
        P("fs", "tp"),
        P("tp"),
        P("tp"),
        P("tp", "fs"),
        P(),
    )
    return jax.shard_map(
        on_device,
        mesh=mesh,
        in_specs=placed,
        out_specs=P(("rep", "fs", "tp"), None),
        check_vma=False,
    )
```

profile of v0, /device:TPU:1, one launch (start us, length us, event | category | flops | bytes accessed | tf_op | source)
XLA Modules:
  0.0 533.2 jit_solution(5803203277212147337)
XLA Ops:
  6.5 0.0 all-gather.3.cloned.1.call-start
  6.5 0.9 convert_element_type.31
  7.5 0.9 convert_element_type.32
  8.4 0.8 pad_maximum_fusion
  9.2 0.0 all-gather.3.cloned.1.call-update
  9.2 0.0 all-gather.5.cloned.1.call-start
  9.3 1.6 convert_element_type.34
  10.8 0.0 all-gather.5.cloned.1.call-update
  10.9 1.2 fusion.11
  12.1 1.2 fusion.13
  13.2 0.4 broadcast_in_dim.2
  13.6 47.1 %all_to_all.10 = bf16[8,96,2048]{2,1,0:T(8,128)(2,1)S(1)} all-to-all(bf16[8,96,2048]{2,1,0:T(8,128)(2,1)S(1)} %broadcast_in_dim.2), channel_id=1, replica_groups=mesh['rep'=2,'fs'=32,'tp'=8] {'tp'}, dimensions={0} | all-to-all | bytes 6291456 | tf_op jit(solution)/shard_map/all_to_all | solution.py:15
  60.7 165.4 %all-gather.3.cloned.1.call-done = bf16[2048,1408]{1,0:T(8,128)(2,1)} async-done(((bf16[64,1408]{1,0:T(8,128)(2,1)}), bf16[2048,1408]{1,0:T(8,128)(2,1)}) %all-gather.3.cloned.1.call-update) | async-done | bytes 5767184 | tf_op jit(solution)/shard_map/all_gather | solution.py:26
  226.1 0.0 copy-start.1
  226.1 0.0 copy-start.2
  226.1 6.8 %fusion = f32[768,704]{0,1:T(8,128)} fusion(bf16[768,2048]{1,0:T(8,128)(2,1)S(1)} %bitcast.5, bf16[2048,1408]{1,0:T(8,128)(2,1)} %all-gather.3.cloned.1.call-done), kind=kOutput, calls=%fused_computation.2 | convolution fusion | flops 2214592512 | bytes 8454144 | tf_op jit(solution)/shard_map/dot_general | solution.py:57
  232.8 215.9 %all-gather.5.cloned.1.call-done = bf16[704,2048]{0,1:T(8,128)(2,1)} async-done(((bf16[704,64]{0,1:T(8,128)(2,1)}), bf16[704,2048]{0,1:T(8,128)(2,1)}) %all-gather.5.cloned.1.call-update) | async-done | bytes 2883600 | tf_op jit(solution)/shard_map/all_gather | solution.py:61
  448.7 0.0 copy-done.1
  448.7 0.0 copy-done.2
  448.7 11.7 %convolution_convert_fusion = bf16[768,2048]{1,0:T(8,128)(2,1)} fusion(bf16[704,2048]{0,1:T(8,128)(2,1)} %all-gather.5.cloned.1.call-done, f32[768,704]{0,1:T(8,128)} %fusion, bf16[768,2048]{1,0:T(8,128)(2,1)S(1)} %bitcast.6, bf16[2048,1408]{1,0:T(8,128)(2,1)} %all-gather.3.cloned.1.call-done, f32[704]{0:T(1024)S(1)} %copy-done.1, f32[704]{0:T(1024)S(1)} %copy-done.2), kind=kOutput, calls=%fused_computation.1 | convolution fusion | flops 4435083264 | bytes 14751232 | tf_op jit(solution)/shard_map/dot_general | solution.py:59
  460.4 64.4 %all_to_all.11 = bf16[8,96,2048]{2,1,0:T(8,128)(2,1)S(1)} all-to-all(bf16[8,96,2048]{2,1,0:T(8,128)(2,1)} %bitcast.7), channel_id=1, replica_groups=mesh['rep'=2,'fs'=32,'tp'=8] {'tp'}, dimensions={0} | all-to-all | bytes 6291456 | tf_op jit(solution)/shard_map/all_to_all | solution.py:41
  524.9 0.0 copy-start
  524.9 0.6 convert_reduce_fusion
  525.4 0.1 copy-done
  525.6 0.8 multiply_convert_fusion.1
  (1 shorter events, 0.0 us)
Async XLA Ops:
  6.5 219.5 %all-gather.3.cloned.1.call-start = ((), (), s32[]{:S(2)}) async-start(), calls=%async_computation.2 | async-start | bytes 5947392 | tf_op jit(solution)/shard_map/all_gather | solution.py:26
  9.2 439.5 %all-gather.5.cloned.1.call-start = ((), (), s32[]{:S(2)}) async-start(), calls=%async_computation.3 | async-start | bytes 3244032 | tf_op jit(solution)/shard_map/all_gather | solution.py:61
  226.1 222.6 %copy-start.1 = (f32[704]{0:T(1024)S(1)}, f32[704]{0:T(1024)}, u32[]{:S(2)}) copy-start(f32[704]{0:T(1024)} %param.13) | copy-start | bytes 8452
  226.1 222.6 %copy-start.2 = (f32[704]{0:T(1024)S(1)}, f32[704]{0:T(1024)}, u32[]{:S(2)}) copy-start(f32[704]{0:T(1024)} %param.12) | copy-start | bytes 8452
  524.9 0.7 copy-start
Sparse Core Ops, SparseCore 0:
  9.4 216.6 all-gather.2
  228.2 220.5 all-gather.4
where the time goes:
time: 534 us; the launch traced here: 533 us
  waiting for transfers between devices  381 us (71%)
  blocking collectives  112 us (21%)
  matrix products  18.5 us (3%)
  between operations  13.4 us (3%)
  other arithmetic  7.93 us (1%)
    all_gather x1, waiting for transfers between devices, on_device(): lax.all_gather(down_weight.astype(jnp.bfloat16), 'fs', axis=1, tiled=True)  216 us
    all_gather x1, waiting for transfers between devices, in_one_piece(): lax.all_gather(both, axis, axis=dim, tiled=True)  165 us
    all_to_all x1, blocking collectives, sum_at_owner(): blocks = lax.all_to_all(cut_along(shard, dim, size), axis, 0, 0, tiled=True)  64.4 us
    all_to_all x1, blocking collectives, sent_to_all(): lax.all_to_all(jnp.broadcast_to(shard[None], (size, *shard.shape)), axis,...  47.1 us
    dot_general x1, matrix products, on_device(): jnp.dot(hidden, lax.all_gather(down_weight.astype(jnp.bfloat16), 'fs', ax...  11.7 us
  transfers between devices with their start and end apart: 2, of which 2 were waited for; matrix products, arithmetic and copies ran while one was open for 2% of the time, Pallas kernels for 0%

commit v1 on v0

--- a/solution.py
+++ b/solution.py
@@ -58,7 +58,12 @@
     hidden = (jax.nn.silu(gate_value * gate_scale) * (up_value * up_scale)).astype(jnp.bfloat16)
     partial_value = jnp.dot(
         hidden,
-        lax.all_gather(down_weight.astype(jnp.bfloat16), "fs", axis=1, tiled=True),
+        jnp.concatenate(
+            lax.all_to_all(
+                jnp.stack([down_weight.astype(jnp.bfloat16)] * lax.axis_size("fs")), "fs", 0, 0
+            ),
+            axis=1,
+        ),
         preferred_element_type=jnp.float32,
     )
     partial_value = partial_value.astype(jnp.bfloat16).astype(jnp.float32)

time: 534 us -> 344 us (0.64)
  the two profiles are of different devices: /device:TPU:1 before, /device:TPU:120 now
where the time goes in v1:
time: 344 us
  waiting for transfers between devices  241 us (70%)
  blocking collectives  42 us (12%)
  starting transfers between devices  18.7 us (5%)
  matrix products  18.5 us (5%)
  between operations  13.5 us (4%)
  other arithmetic  5.43 us (2%)
  local copies, waits for them, and re-layouts  4.26 us (1%)
    all_gather x1, waiting for transfers between devices, in_one_piece(): lax.all_gather(both, axis, axis=dim, tiled=True)  205 us
    all_to_all x1, blocking collectives, sum_at_owner(): blocks = lax.all_to_all(cut_along(shard, dim, size), axis, 0, 0, tiled=True)  42 us
    all_to_all x1, waiting for transfers between devices, sent_to_all(): lax.all_to_all(jnp.broadcast_to(shard[None], (size, *shard.shape)), axis,...  36.6 us
    all_to_all x1, starting transfers between devices, on_device(): lax.all_to_all(jnp.stack([down_weight.astype(jnp.bfloat16)] * lax.axis_si...  14.2 us
    dot_general x1, matrix products, on_device(): jnp.dot(hidden, jnp.concatenate(lax.all_to_all(jnp.stack([down_weight.ast...  11.7 us
  transfers between devices with their start and end apart: 3, of which 2 were waited for; matrix products, arithmetic and copies ran while one was open for 3% of the time, Pallas kernels for 0%

profile of v1, /device:TPU:120, one launch (start us, length us, event | category | flops | bytes accessed | tf_op | source)
XLA Modules:
  0.0 343.8 jit_solution(4646088823671281280)
XLA Ops:
  6.5 1.2 fusion.11
  7.7 1.2 fusion.13
  8.9 2.1 broadcast_in_dim.2
  11.0 0.0 copy-start
  11.0 0.0 copy-start.1
  11.0 4.4 %all-to-all-start = ((bf16[8,96,2048]{2,1,0:T(8,128)(2,1)}), bf16[8,96,2048]{2,1,0:T(8,128)(2,1)S(1)}, u32[]{:S(2)}, u32[]{:S(2)}) async-start(bf16[8,96,2048]{2,1,0:T(8,128)(2,1)} %broadcast_in_dim.2), calls=%async_computation | async-start | bytes 6291456 | tf_op jit(solution)/shard_map/all_to_all | solution.py:15
  15.4 0.0 all-gather.2.cloned.1.call-start
  15.5 0.0 copy-done
  15.5 0.0 copy-done.1
  15.5 0.8 pad_maximum_fusion
  16.3 0.0 all-gather.2.cloned.1.call-update
  16.3 0.9 convert_element_type.34
  17.3 36.6 %all-to-all-done = bf16[8,96,2048]{2,1,0:T(8,128)(2,1)S(1)} async-done(((bf16[8,96,2048]{2,1,0:T(8,128)(2,1)}), bf16[8,96,2048]{2,1,0:T(8,128)(2,1)S(1)}, u32[]{:S(2)}, u32[]{:S(2)}) %all-to-all-start) | async-done | bytes 3145760 | tf_op jit(solution)/shard_map/all_to_all | solution.py:15
  53.8 2.0 stack.2
  55.8 14.2 %all-to-all-start.1 = ((bf16[32,704,64]{1,2,0:T(8,128)(2,1)}), bf16[32,704,64]{1,2,0:T(8,128)(2,1)}, u32[]{:S(2)}, u32[]{:S(2)}) async-start(bf16[32,704,64]{1,2,0:T(8,128)(2,1)} %stack.2), calls=%async_computation.1 | async-start | bytes 6291456 | tf_op jit(solution)/shard_map/all_to_all | solution.py:62
  70.1 204.9 %all-gather.2.cloned.1.call-done = bf16[2048,1408]{1,0:T(8,128)(2,1)} async-done(((bf16[64,1408]{1,0:T(8,128)(2,1)}), bf16[2048,1408]{1,0:T(8,128)(2,1)}) %all-gather.2.cloned.1.call-update) | async-done | bytes 5767184 | tf_op jit(solution)/shard_map/all_gather | solution.py:26
  275.0 0.0 copy-start.3
  275.0 0.0 copy-start.4
  275.0 6.7 %fusion = f32[768,704]{0,1:T(8,128)} fusion(bf16[768,2048]{1,0:T(8,128)(2,1)S(1)} %bitcast.8, bf16[2048,1408]{1,0:T(8,128)(2,1)} %all-gather.2.cloned.1.call-done), kind=kOutput, calls=%fused_computation.2 | convolution fusion | flops 2214592512 | bytes 8454144 | tf_op jit(solution)/shard_map/dot_general | solution.py:57
  281.7 0.0 all-to-all-done.1
  281.7 0.0 copy-done.3
  281.7 0.0 copy-done.4
  281.7 11.7 %convolution_convert_fusion = bf16[768,2048]{1,0:T(8,128)(2,1)} fusion(bf16[704,2048]{0,1:T(8,128)(2,1)} %bitcast.2, f32[768,704]{0,1:T(8,128)} %fusion, bf16[768,2048]{1,0:T(8,128)(2,1)S(1)} %bitcast.9, bf16[2048,1408]{1,0:T(8,128)(2,1)} %all-gather.2.cloned.1.call-done, f32[704]{0:T(1024)S(1)} %copy-done.3, f32[704]{0:T(1024)S(1)} %copy-done.4), kind=kOutput, calls=%fused_computation.1 | convolution fusion | flops 4435083264 | bytes 14751232 | tf_op jit(solution)/shard_map/dot_general | solution.py:59
  293.5 42.0 %all_to_all.15 = bf16[8,96,2048]{2,1,0:T(8,128)(2,1)S(1)} all-to-all(bf16[8,96,2048]{2,1,0:T(8,128)(2,1)} %bitcast.10), channel_id=1, replica_groups=mesh['rep'=2,'fs'=32,'tp'=8] {'tp'}, dimensions={0} | all-to-all | bytes 6291456 | tf_op jit(solution)/shard_map/all_to_all | solution.py:41
  335.5 0.0 copy-start.2
  335.5 0.5 convert_reduce_fusion
  336.0 0.1 copy-done.2
  336.2 0.8 multiply_convert_fusion.1
  (3 shorter events, 0.0 us)
Async XLA Ops:
  11.0 4.5 %copy-start = (f32[64,704]{1,0:T(8,128)S(1)}, f32[64,704]{1,0:T(8,128)}, u32[]{:S(2)}) copy-start(f32[64,704]{1,0:T(8,128)} %param.11) | copy-start | bytes 540676
  11.0 4.5 %copy-start.1 = (f32[64,704]{1,0:T(8,128)S(1)}, f32[64,704]{1,0:T(8,128)}, u32[]{:S(2)}) copy-start(f32[64,704]{1,0:T(8,128)} %param.10) | copy-start | bytes 540676
  11.0 42.8 %all-to-all-start = ((bf16[8,96,2048]{2,1,0:T(8,128)(2,1)}), bf16[8,96,2048]{2,1,0:T(8,128)(2,1)S(1)}, u32[]{:S(2)}, u32[]{:S(2)}) async-start(bf16[8,96,2048]{2,1,0:T(8,128)(2,1)} %broadcast_in_dim.2), calls=%async_computation | async-start | bytes 6291456 | tf_op jit(solution)/shard_map/all_to_all | solution.py:15
  15.4 259.5 %all-gather.2.cloned.1.call-start = ((), (), s32[]{:S(2)}) async-start(), calls=%async_computation.3 | async-start | bytes 5947392 | tf_op jit(solution)/shard_map/all_gather | solution.py:26
  55.8 225.9 %all-to-all-start.1 = ((bf16[32,704,64]{1,2,0:T(8,128)(2,1)}), bf16[32,704,64]{1,2,0:T(8,128)(2,1)}, u32[]{:S(2)}, u32[]{:S(2)}) async-start(bf16[32,704,64]{1,2,0:T(8,128)(2,1)} %stack.2), calls=%async_computation.1 | async-start | bytes 6291456 | tf_op jit(solution)/shard_map/all_to_all | solution.py:62
  275.0 6.8 %copy-start.3 = (f32[704]{0:T(1024)S(1)}, f32[704]{0:T(1024)}, u32[]{:S(2)}) copy-start(f32[704]{0:T(1024)} %param.13) | copy-start | bytes 8452
  275.0 6.8 %copy-start.4 = (f32[704]{0:T(1024)S(1)}, f32[704]{0:T(1024)}, u32[]{:S(2)}) copy-start(f32[704]{0:T(1024)} %param.12) | copy-start | bytes 8452
  335.5 0.7 copy-start.2
Sparse Core Ops, SparseCore 0:
  18.3 256.6 all-gather.1
